TPU v7x, 32 devices: a whole 2x2x4 slice. The times are simulated.
32 devices in a mesh: grp: 2 (over y), sp: 4 (over z), tp: 4 (over x, core).
Axes of the slice: x: 2, y: 2, z: 4, core: 2. Of those that a mesh axis runs over, the one named last changes fastest.
Arguments:
- source: bfloat16 [4096, 2048], P(('grp', 'sp', 'tp')), parts along dimension 0, may hold values from -8 to 8
- target: bfloat16 [1024, 2048], P(('grp', 'sp', 'tp')), parts along dimension 0, may hold values from -8 to 8
- source_gain: float32 [2048], replicated, may hold values from 0.1 to 1.9
- attend_gain: float32 [2, 2048], replicated, may hold values from 0.1 to 1.9
- query_weight: bfloat16 [2, 2048, 2048], P(None, None, 'tp'), may hold values from -4 to 4
- key_weight: bfloat16 [2, 2048, 2048], P(None, None, 'tp'), may hold values from -4 to 4
- value_weight: bfloat16 [2, 2048, 2048], P(None, None, 'tp'), may hold values from -0.125 to 0.125
- out_weight: bfloat16 [2, 2048, 2048], P(None, 'tp'), may hold values from -3 to 3
- mixer_gain: float32 [2048], replicated, may hold values from 0.1 to 1.9
- gate_weight: bfloat16 [2048, 2816], P(None, 'tp'), may hold values from -0.125 to 0.125
- up_weight: bfloat16 [2048, 2816], P(None, 'tp'), may hold values from -0.125 to 0.125
- gate_taps: float32 [3, 2816], P(None, 'tp'), may hold values from -3 to 3
- up_taps: float32 [3, 2816], P(None, 'tp'), may hold values from -3 to 3
- down_weight: bfloat16 [2816, 2048], P('tp'), may hold values from -0.109375 to 0.109375
- final_gain: float32 [2048], replicated, may hold values from 0.1 to 1.9
Outputs:
- result: bfloat16 [1024, 2048], P(('grp', 'sp', 'tp')), parts along dimension 0
There are 2 independent parts, one for each index of `grp`. A program takes and returns all parts, laid end to end along the dimension named above; an argument that names none is the same for every part. Nothing has to cross between parts.
All inputs are finite; a program needn't handle non-finite values.
Results may differ from a plain program's by a relative error of at most 0.04.
Values may be sent and summed in bfloat16 or wider, within the bound.
A program may use at most 128 MiB of HBM per device.

v0:
```python
import jax
import jax.numpy as jnp
from jax import lax
from jax.sharding import PartitionSpec as P

HD = 256


EPS = 1e-06


def shifted(value, axis, steps):
    count = lax.axis_size(axis)
    first, last = (max(0, -steps), min(count, count - steps))
    return lax.ppermute(value, axis, [(source, source + steps) for source in range(first, last)])


def normed_rows(rows, gain):
    wide = rows.astype(jnp.float32)
    return wide * lax.rsqrt(jnp.mean(wide * wide, axis=-1, keepdims=True) + EPS) * gain


def attend_layer(residual, key_rows, value_rows, gain, w_query, w_out):
    width = w_query.shape[1]
    heads_here = width // HD
    head_scale = HD ** (-0.5)
    normed = normed_rows(residual, gain).astype(jnp.bfloat16)
    query_block = jnp.dot(
        lax.all_gather(normed, "tp", axis=0, tiled=True),
        w_query,
        preferred_element_type=jnp.float32,
    ).astype(jnp.bfloat16)
    row_count = query_block.shape[0]
    key_heads = key_rows.reshape(-1, heads_here, HD)
    value_heads = value_rows.reshape(-1, heads_here, HD)
    every_query = lax.all_gather(query_block, "sp", axis=0, tiled=True)
    every_heads = every_query.reshape(-1, heads_here, HD)
    scores = (
        jnp.einsum("thd,shd->hts", every_heads, key_heads, preferred_element_type=jnp.float32)
        * head_scale
    )
    highest = lax.pmax(jnp.max(scores, axis=-1), "sp")
    raised = jnp.exp(scores - highest[:, :, None])
    weighted = jnp.einsum(
        "hts,shd->thd", raised.astype(jnp.bfloat16), value_heads, preferred_element_type=jnp.float32
    )
    row_totals = jnp.sum(raised, axis=-1).T
    own_sums, own_totals = (
        lax.psum_scatter(
            weighted.astype(jnp.bfloat16), "sp", scatter_dimension=0, tiled=True
        ).astype(jnp.float32),
        lax.psum_scatter(
            row_totals.astype(jnp.bfloat16), "sp", scatter_dimension=0, tiled=True
        ).astype(jnp.float32),
    )
    attended = (own_sums / own_totals[:, :, None]).reshape(row_count, width).astype(jnp.bfloat16)
    return lax.psum_scatter(
        jnp.dot(attended, w_out, preferred_element_type=jnp.float32).astype(jnp.bfloat16),
        "tp",
        scatter_dimension=0,
        tiled=True,
    ).astype(jnp.float32)


def body(
    source,
    target,
    source_gain,
    attend_gain,
    query_weight,
    key_weight,
    value_weight,
    out_weight,
    mixer_gain,
    gate_weight,
    up_weight,
    gate_taps,
    up_taps,
    down_weight,
    final_gain,
):
    width = query_weight.shape[2]
    source_normed = normed_rows(source, source_gain).astype(jnp.bfloat16)
    joined_weights = jnp.concatenate(
        [key_weight[0], value_weight[0], key_weight[1], value_weight[1]], axis=1
    )
    projected = jnp.dot(
        lax.all_gather(source_normed, "tp", axis=0, tiled=True),
        joined_weights,
        preferred_element_type=jnp.float32,
    ).astype(jnp.bfloat16)
    residual = target.astype(jnp.float32)
    for layer_number in range(2):
        key_rows = projected[:, 2 * layer_number * width : (2 * layer_number + 1) * width]
        value_rows = projected[:, (2 * layer_number + 1) * width : (2 * layer_number + 2) * width]
        residual = residual + attend_layer(
            residual,
            key_rows,
            value_rows,
            attend_gain[layer_number],
            query_weight[layer_number],
            out_weight[layer_number],
        )
    mixed = normed_rows(residual, mixer_gain).astype(jnp.bfloat16)
    portion = lax.all_gather(mixed, "tp", axis=0, tiled=True)
    gate_part = jnp.dot(portion, gate_weight, preferred_element_type=jnp.float32)
    up_part = jnp.dot(portion, up_weight, preferred_element_type=jnp.float32)
    lifted = jnp.concatenate([gate_part, up_part], axis=1).astype(jnp.bfloat16)
    earlier = shifted(lifted[-2:], "sp", 1)
    padded = jnp.concatenate([earlier, lifted], axis=0).astype(jnp.float32)
    all_taps = jnp.concatenate([gate_taps, up_taps], axis=1)
    convolved = all_taps[0] * padded[:-2] + all_taps[1] * padded[1:-1] + all_taps[2] * padded[2:]
    inner_units = gate_weight.shape[1]
    hidden = (jax.nn.silu(convolved[:, :inner_units]) * convolved[:, inner_units:]).astype(
        jnp.bfloat16
    )
    residual = residual + lax.psum_scatter(
        jnp.dot(hidden, down_weight, preferred_element_type=jnp.float32).astype(jnp.bfloat16),
        "tp",
        scatter_dimension=0,
        tiled=True,
    ).astype(jnp.float32)
    return normed_rows(residual, final_gain).astype(jnp.bfloat16)


def solution(mesh):
    placed = (
        P(("grp", "sp", "tp"), None),
        P(("grp", "sp", "tp"), None),
        P(),
        P(),
        P(None, None, "tp"),
        P(None, None, "tp"),
        P(None, None, "tp"),
        P(None, "tp", None),
        P(),
        P(None, "tp"),
        P(None, "tp"),
        P(None, "tp"),
        P(None, "tp"),
        P("tp", None),
        P(),
    )
    return jax.shard_map(
        body, mesh=mesh, in_specs=placed, out_specs=P(("grp", "sp", "tp"), None), check_vma=False
    )
```

profile of v0, /device:TPU:0, one launch (start us, length us, event | category | flops | bytes accessed | tf_op | source)
XLA Modules:
  0.0 301.9 jit_solution(114304977294703288)
XLA Ops:
  7.9 2.1 fusion.33
  10.4 8.8 %all_gather.19 = bf16[128,2048]{1,0:T(8,128)(2,1)S(1)} all-gather(bf16[32,2048]{1,0:T(8,128)(2,1)S(1)} %fusion.55), channel_id=1, replica_groups=mesh['grp'=2,'sp'=4,'tp'=4] {'tp'}, dimensions={0}, use_global_device_ids=true | all-gather | bytes 655360 | tf_op jit(solution)/shard_map/all_gather | solution.py:29
  19.2 2.2 fusion.25
  21.3 16.3 %all_gather.20 = bf16[512,512]{1,0:T(8,128)(2,1)S(1)} all-gather(bf16[128,512]{1,0:T(8,128)(2,1)S(1)} %fusion.25), channel_id=1, replica_groups=mesh['grp'=2,'sp'=4,'tp'=4] {'sp'}, dimensions={0}, use_global_device_ids=true | all-gather | bytes 655360 | tf_op jit(solution)/shard_map/all_gather | solution.py:36
  37.7 4.9 %slice_bitcast_fusion.2 = (bf16[2048,512]{1,0:T(8,128)(2,1)}, bf16[2048,512]{1,0:T(8,128)(2,1)}, bf16[2048,512]{1,0:T(8,128)(2,1)}, bf16[2048,512]{1,0:T(8,128)(2,1)}) fusion(bf16[2,2048,512]{2,1,0:T(8,128)(2,1)S(1)} %copy-done.3, bf16[2,2048,512]{2,1,0:T(8,128)(2,1)} %param.20), kind=kLoop, calls=%fused_computation.26 | loop fusion | bytes 16777216 | tf_op jit(solution)/shard_map/squeeze | solution.py:85
  42.6 8.9 %fusion.8 = bf16[512,2048]{1,0:T(8,128)(2,1)S(1)} fusion(bf16[512,2048]{1,0:T(8,128)(2,1)} %all-gather.2.cloned.1.call-done, bf16[2048,512]{1,0:T(8,128)(2,1)} %get-tuple-element.11, bf16[2048,512]{1,0:T(8,128)(2,1)} %get-tuple-element.22, bf16[2048,512]{1,0:T(8,128)(2,1)} %get-tuple-element.10, bf16[2048,512]{1,0:T(8,128)(2,1)} %get-tuple-element.23), kind=kOutput, calls=%fused_computation.8 | convolution fusion | flops 4329570304 | bytes 12582912 | tf_op jit(solution)/shard_map/dot_general | solution.py:87
  52.7 1.8 multiply_reduce_fusion.1
  54.5 12.1 %pmax.14 = f32[2,512]{1,0:T(2,128)S(1)} all-reduce(f32[2,512]{1,0:T(2,128)S(1)} %get-tuple-element.18), channel_id=1, replica_groups=mesh['grp'=2,'sp'=4,'tp'=4] {'sp'}, use_global_device_ids=true, to_apply=%region_3.0 | all-reduce | flops 1024 | bytes 8192 | tf_op jit(solution)/shard_map/pmax | solution.py:42
  67.9 2.0 fusion.21
  70.7 2.9 convolution_convert_fusion.4
  73.6 2.1 copy.44
  75.8 12.4 %reduce-scatter.24.cloned.1.call-done = bf16[128,2]{1,0:T(8,128)(2,1)} async-done(((bf16[512,2]{1,0:T(8,128)(2,1)}), bf16[128,2]{1,0:T(8,128)(2,1)}) %reduce-scatter.24.cloned.1.call-update) | async-done | bytes 528
  89.0 21.5 %reduce-scatter.22.cloned.1.call-done = bf16[128,512]{1,0:T(8,128)(2,1)} async-done(((bf16[512,512]{1,0:T(8,128)(2,1)}), bf16[128,512]{1,0:T(8,128)(2,1)}) %reduce-scatter.22.cloned.1.call-update) | async-done | bytes 131088
  111.5 2.9 convolution_convert_fusion.2
  115.7 18.8 %reduce-scatter.16.cloned.1.call-done = bf16[32,2048]{1,0:T(8,128)(2,1)} async-done(((bf16[128,2048]{1,0:T(8,128)(2,1)}), bf16[32,2048]{1,0:T(8,128)(2,1)}) %reduce-scatter.16.cloned.1.call-update) | async-done | bytes 131088 | tf_op jit(solution)/shard_map/reduce_scatter | solution.py:57
  136.5 6.6 %all_gather.21 = bf16[128,2048]{1,0:T(8,128)(2,1)S(1)} all-gather(bf16[32,2048]{1,0:T(8,128)(2,1)S(1)} %multiply_convert_fusion.2), channel_id=1, replica_groups=mesh['grp'=2,'sp'=4,'tp'=4] {'tp'}, dimensions={0}, use_global_device_ids=true | all-gather | bytes 655360 | tf_op jit(solution)/shard_map/all_gather | solution.py:29
  143.1 2.1 fusion.28
  145.2 16.1 %all_gather.22 = bf16[512,512]{1,0:T(8,128)(2,1)S(1)} all-gather(bf16[128,512]{1,0:T(8,128)(2,1)S(1)} %fusion.28), channel_id=1, replica_groups=mesh['grp'=2,'sp'=4,'tp'=4] {'sp'}, dimensions={0}, use_global_device_ids=true | all-gather | bytes 655360 | tf_op jit(solution)/shard_map/all_gather | solution.py:36
  161.3 1.8 multiply_reduce_fusion
  163.1 12.2 %pmax.15 = f32[2,512]{1,0:T(2,128)S(1)} all-reduce(f32[2,512]{1,0:T(2,128)S(1)} %get-tuple-element.20), channel_id=1, replica_groups=mesh['grp'=2,'sp'=4,'tp'=4] {'sp'}, use_global_device_ids=true, to_apply=%region_10.0 | all-reduce | flops 1024 | bytes 8192 | tf_op jit(solution)/shard_map/pmax | solution.py:42
  175.3 2.0 fusion.23
  178.2 2.9 convolution_convert_fusion.3
  181.1 2.1 copy.46
  183.2 12.2 %reduce-scatter.28.cloned.1.call-done = bf16[128,2]{1,0:T(8,128)(2,1)} async-done(((bf16[512,2]{1,0:T(8,128)(2,1)}), bf16[128,2]{1,0:T(8,128)(2,1)}) %reduce-scatter.28.cloned.1.call-update) | async-done | bytes 528
  196.3 21.4 %reduce-scatter.26.cloned.1.call-done = bf16[128,512]{1,0:T(8,128)(2,1)} async-done(((bf16[512,512]{1,0:T(8,128)(2,1)}), bf16[128,512]{1,0:T(8,128)(2,1)}) %reduce-scatter.26.cloned.1.call-update) | async-done | bytes 131088
  218.7 2.9 convolution_convert_fusion.1
  221.6 20.0 %reduce-scatter.18.cloned.1.call-done = bf16[32,2048]{1,0:T(8,128)(2,1)} async-done(((bf16[128,2048]{1,0:T(8,128)(2,1)}), bf16[32,2048]{1,0:T(8,128)(2,1)}) %reduce-scatter.18.cloned.1.call-update) | async-done | bytes 131088 | tf_op jit(solution)/shard_map/reduce_scatter | solution.py:57
  243.7 6.9 %all_gather.23 = bf16[128,2048]{1,0:T(8,128)(2,1)S(1)} all-gather(bf16[32,2048]{1,0:T(8,128)(2,1)S(1)} %multiply_convert_fusion.1), channel_id=1, replica_groups=mesh['grp'=2,'sp'=4,'tp'=4] {'tp'}, dimensions={0}, use_global_device_ids=true | all-gather | bytes 655360 | tf_op jit(solution)/shard_map/all_gather | solution.py:105
  250.6 2.7 convolution_convert_fusion.5
  254.5 3.4 %collective-permute-start = (bf16[2,1408]{0,1:T(8,128)(2,1)S(1)}, bf16[2,1408]{0,1:T(8,128)(2,1)S(1)}, u32[]{:S(2)}, u32[]{:S(2)}) collective-permute-start(bf16[2,1408]{0,1:T(8,128)(2,1)S(1)} %pad_maximum_fusion), channel_id=1, source_target_pairs={{0,4},{4,8},{8,12},{1,5},{5,9},{9,13},{2,6},{6,10},{10,14},{3,7},{... | collective-permute-start | bytes 16904 | tf_op jit(solution)/shard_map/ppermute | solution.py:15
  258.0 8.0 %collective-permute-done = bf16[2,1408]{0,1:T(8,128)(2,1)S(1)} collective-permute-done((bf16[2,1408]{0,1:T(8,128)(2,1)S(1)}, bf16[2,1408]{0,1:T(8,128)(2,1)S(1)}, u32[]{:S(2)}, u32[]{:S(2)}) %collective-permute-start) | collective-permute-done | bytes 5664 | tf_op jit(solution)/shard_map/ppermute | solution.py:15
  269.0 23.3 %reduce-scatter.20.cloned.1.call-done = bf16[32,2048]{1,0:T(8,128)(2,1)} async-done(((bf16[128,2048]{1,0:T(8,128)(2,1)}), bf16[32,2048]{1,0:T(8,128)(2,1)}) %reduce-scatter.20.cloned.1.call-update) | async-done | bytes 131088 | tf_op jit(solution)/shard_map/reduce_scatter | solution.py:117
  (75 shorter events, 22.2 us)
Async XLA Ops:
  6.5 261.0 %copy-start = (bf16[704,2048]{1,0:T(8,128)(2,1)S(1)}, bf16[704,2048]{1,0:T(8,128)(2,1)}, u32[]{:S(2)}) copy-start(bf16[704,2048]{1,0:T(8,128)(2,1)} %param.28) | copy-start | bytes 8650756
  6.5 3.5 %copy-start.1 = (bf16[32,2048]{1,0:T(8,128)(2,1)S(1)}, bf16[32,2048]{1,0:T(8,128)(2,1)}, u32[]{:S(2)}) copy-start(bf16[32,2048]{1,0:T(8,128)(2,1)} %param.16) | copy-start | bytes 393220
  6.5 3.7 %copy-start.7 = (f32[2,2048]{1,0:T(2,128)S(1)}, f32[2,2048]{1,0:T(2,128)}, u32[]{:S(2)}) copy-start(f32[2,2048]{1,0:T(2,128)} %param.18) | copy-start | bytes 49156
  6.5 36.1 %all-gather.2.cloned.1.call-start = ((), (), s32[]{:S(2)}) async-start(), calls=%async_computation.7 | async-start | bytes 2621440 | tf_op jit(solution)/shard_map/all_gather | solution.py:88
  10.0 78.1 %reduce-scatter.24.cloned.1.call-start = ((), (), s32[]{:S(2)}) async-start(), calls=%async_computation.12 | async-start | bytes 163840
  10.4 27.3 %copy-start.3 = (bf16[2,2048,512]{2,1,0:T(8,128)(2,1)S(1)}, bf16[2,2048,512]{2,1,0:T(8,128)(2,1)}, u32[]{:S(2)}) copy-start(bf16[2,2048,512]{2,1,0:T(8,128)(2,1)} %param.21) | copy-start | bytes 12582916
  70.7 39.7 %reduce-scatter.22.cloned.1.call-start = ((), (), s32[]{:S(2)}) async-start(), calls=%async_computation.11 | async-start | bytes 655360
  75.7 58.7 %reduce-scatter.16.cloned.1.call-start = ((), (), s32[]{:S(2)}) async-start(), calls=%async_computation.8 | async-start | bytes 655360 | tf_op jit(solution)/shard_map/reduce_scatter | solution.py:57
  114.4 81.1 %reduce-scatter.28.cloned.1.call-start = ((), (), s32[]{:S(2)}) async-start(), calls=%async_computation.14 | async-start | bytes 163840
  143.1 18.2 %copy-start.6 = (bf16[512,512]{1,0:T(8,128)(2,1)S(1)}, bf16[512,512]{1,0:T(8,128)(2,1)}, u32[]{:S(2)}) copy-start(bf16[512,512]{1,0:T(8,128)(2,1)} %get-tuple-element.13) | copy-start | bytes 1572868
  178.1 39.5 %reduce-scatter.26.cloned.1.call-start = ((), (), s32[]{:S(2)}) async-start(), calls=%async_computation.13 | async-start | bytes 655360
  183.1 58.5 %copy-start.2 = (bf16[32,2048]{1,0:T(8,128)(2,1)S(1)}, bf16[32,2048]{1,0:T(8,128)(2,1)}, u32[]{:S(2)}) copy-start(bf16[32,2048]{1,0:T(8,128)(2,1)} %reduce-scatter.16.cloned.1.call-done) | copy-start | bytes 393220
  183.2 58.4 %reduce-scatter.18.cloned.1.call-start = ((), (), s32[]{:S(2)}) async-start(), calls=%async_computation.9 | async-start | bytes 655360 | tf_op jit(solution)/shard_map/reduce_scatter | solution.py:57
  196.3 46.4 %copy-start.10 = (f32[2048]{0:T(1024)S(1)}, f32[2048]{0:T(1024)}, u32[]{:S(2)}) copy-start(f32[2048]{0:T(1024)} %param.23) | copy-start | bytes 24580
  221.6 70.7 %reduce-scatter.20.cloned.1.call-start = ((), (), s32[]{:S(2)}) async-start(), calls=%async_computation.10 | async-start | bytes 655360 | tf_op jit(solution)/shard_map/reduce_scatter | solution.py:117
  243.7 9.7 %copy-start.4 = (bf16[2048,704]{0,1:T(8,128)(2,1)S(1)}, bf16[2048,704]{0,1:T(8,128)(2,1)}, u32[]{:S(2)}) copy-start(bf16[2048,704]{0,1:T(8,128)(2,1)} %param.24) | copy-start | bytes 8650756
  253.4 4.5 %copy-start.8 = (f32[3,704]{1,0:T(4,128)S(1)}, f32[3,704]{1,0:T(4,128)}, u32[]{:S(2)}) copy-start(f32[3,704]{1,0:T(4,128)} %param.27) | copy-start | bytes 25348
  253.4 4.5 %copy-start.9 = (f32[3,704]{1,0:T(4,128)S(1)}, f32[3,704]{1,0:T(4,128)}, u32[]{:S(2)}) copy-start(f32[3,704]{1,0:T(4,128)} %param.26) | copy-start | bytes 25348
  254.5 11.6 %collective-permute-start = (bf16[2,1408]{0,1:T(8,128)(2,1)S(1)}, bf16[2,1408]{0,1:T(8,128)(2,1)S(1)}, u32[]{:S(2)}, u32[]{:S(2)}) collective-permute-start(bf16[2,1408]{0,1:T(8,128)(2,1)S(1)} %pad_maximum_fusion), channel_id=1, source_target_pairs={{0,4},{4,8},{8,12},{1,5},{5,9},{9,13},{2,6},{6,10},{10,14},{3,7},{... | collective-permute-start | bytes 16904 | tf_op jit(solution)/shard_map/ppermute | solution.py:15
  267.5 24.8 %copy-start.5 = (bf16[32,2048]{1,0:T(8,128)(2,1)S(1)}, bf16[32,2048]{1,0:T(8,128)(2,1)}, u32[]{:S(2)}) copy-start(bf16[32,2048]{1,0:T(8,128)(2,1)} %reduce-scatter.18.cloned.1.call-done) | copy-start | bytes 393220
  267.5 25.9 %copy-start.11 = (f32[2048]{0:T(1024)S(1)}, f32[2048]{0:T(1024)}, u32[]{:S(2)}) copy-start(f32[2048]{0:T(1024)} %param.29) | copy-start | bytes 24580
Sparse Core Ops, SparseCore 0:
  10.1 25.2 all-gather.1
  70.8 17.2 reduce-scatter.23
  90.4 19.9 reduce-scatter.21
  114.5 19.9 reduce-scatter.15
  178.2 17.1 reduce-scatter.27
  197.6 20.0 reduce-scatter.25
  221.7 19.8 reduce-scatter.17
  269.1 23.1 reduce-scatter.19
where the time goes:
time: 303 us; the launch traced here: 302 us
  waiting for transfers between devices  138 us (46%)
  blocking collectives  79 us (26%)
  matrix products  33.5 us (11%)
  local copies, waits for them, and re-layouts  18.1 us (6%)
  other arithmetic  16.3 us (5%)
  between operations  13.8 us (5%)
  starting transfers between devices  3.69 us (1%)
    unnamed x12, waiting for transfers between devices  67.5 us
    reduce_scatter x2, waiting for transfers between devices, attend_layer(): lax.psum_scatter(jnp.dot(attended, w_out, preferred_element_type=jnp.floa...  38.7 us
    all_gather x2, blocking collectives, attend_layer(): every_query = lax.all_gather(query_block, 'sp', axis=0, tiled=True)  32.4 us
    pmax x2, blocking collectives, attend_layer(): highest = lax.pmax(jnp.max(scores, axis=-1), 'sp')  24.3 us
    reduce_scatter x1, waiting for transfers between devices, body(): lax.psum_scatter(jnp.dot(hidden, down_weight, preferred_element_type=jnp....  23.3 us
    all_gather x2, blocking collectives, attend_layer(): lax.all_gather(normed, 'tp', axis=0, tiled=True)  15.4 us
    unnamed x32, local copies, waits for them, and re-layouts  9.48 us
    dot_general x1, matrix products, body(): jnp.dot(lax.all_gather(source_normed, 'tp', axis=0, tiled=True), joined_w...  8.9 us
  transfers between devices with their start and end apart: 9, of which 8 were waited for; matrix products, arithmetic and copies ran while one was open for 7% of the time, Pallas kernels for 0%

commit v1 on v0

v1 whole, which is shorter than its diff:
```python
import functools

import jax
import jax.numpy as jnp
from jax import lax
from jax.experimental import pallas as pl
from jax.experimental.pallas import tpu as pltpu
from jax.sharding import PartitionSpec as P

HD = 256
EPS = 1e-06
TILE = 256
STAT_ROWS = 8
LANES = 128
MESH = pl.DeviceIdType.MESH
BF = jnp.bfloat16
F32 = jnp.float32


def normed_rows(wide, gain):
    return wide * lax.rsqrt(jnp.mean(wide * wide, axis=-1, keepdims=True) + EPS) * gain


def mm(a, b):
    return jnp.dot(a, b, preferred_element_type=F32)


def kernel(
    n,
    S,
    source,
    target,
    source_gain,
    attend_gain,
    query_weight,
    key_weight,
    value_weight,
    out_weight,
    mixer_gain,
    gate_weight,
    up_weight,
    gate_taps,
    up_taps,
    down_weight,
    final_gain,
    result,
    sv,
    tv,
    wq,
    wkv,
    wo,
    wg,
    wu,
    wd,
    xs,
    xt,
    kv,
    qall,
    osend,
    orecv,
    ssend,
    srecv,
    pf,
    att,
    p1s,
    p1r,
    p2s,
    p2r,
    hs,
    hr,
    gpad,
    upad,
    hid,
    residual,
    load_sem,
    w_sem,
    ag_send,
    ag_recv,
    q_send,
    q_recv,
    r_send,
    r_recv,
    s_send,
    s_recv,
    p1_send,
    p1_recv,
    p2_send,
    p2_recv,
    h_send,
    h_recv,
):
    X = n // 2
    Rs, D = source.shape
    Rt = target.shape[0]
    W = wq.shape[2]
    T = n * Rt
    heads = W // HD
    F = wg.shape[1]
    scale = HD ** (-0.5)
    t = lax.axis_index("tp")
    s = lax.axis_index("sp")
    x = lax.div(t, 2)
    c = lax.rem(t, 2)
    other = 1 - c
    peer = x * 2 + other
    pending = []

    def tp_at(k):
        return lax.rem(x + k, X)

    def tp_from(k):
        return lax.rem(x + X - k, X)

    def sp_at(i):
        return lax.rem(s + i, S)

    def remote(src, dst, ss, rs, axis, where):
        return pltpu.make_async_remote_copy(
            src_ref=src,
            dst_ref=dst,
            send_sem=ss,
            recv_sem=rs,
            device_id={axis: where},
            device_id_type=MESH,
        )

    def launch(copy):
        copy.start()
        pending.append(copy)

    barrier = pltpu.get_barrier_semaphore()
    pl.semaphore_signal(barrier, inc=1, device_id={"tp": peer}, device_id_type=MESH)
    for k in range(1, X):
        pl.semaphore_signal(
            barrier, inc=1, device_id={"tp": tp_at(k) * 2 + c}, device_id_type=MESH
        )
    for i in range(1, S):
        pl.semaphore_signal(barrier, inc=1, device_id={"sp": sp_at(i)}, device_id_type=MESH)

    load_t = pltpu.make_async_copy(target, tv, load_sem.at[0])
    load_s = pltpu.make_async_copy(source, sv, load_sem.at[1])
    load_t.start()
    load_s.start()
    load_q = [pltpu.make_async_copy(query_weight.at[l], wq.at[l], w_sem.at[l]) for l in range(2)]
    load_kv = []
    for l in range(2):
        load_kv.append(
            [
                pltpu.make_async_copy(key_weight.at[l], wkv.at[2 * l], w_sem.at[2 + 2 * l]),
                pltpu.make_async_copy(value_weight.at[l], wkv.at[2 * l + 1], w_sem.at[3 + 2 * l]),
            ]
        )
    load_o = [pltpu.make_async_copy(out_weight.at[l], wo.at[l], w_sem.at[6 + l]) for l in range(2)]
    load_m = [
        pltpu.make_async_copy(gate_weight, wg, w_sem.at[8]),
        pltpu.make_async_copy(up_weight, wu, w_sem.at[9]),
        pltpu.make_async_copy(down_weight, wd, w_sem.at[10]),
    ]
    for copy in [load_q[0], *load_kv[0], *load_kv[1], load_o[0], load_q[1], load_o[1], *load_m]:
        copy.start()

    def gather_start(a, buf):
        for k in range(1, X):
            launch(
                remote(
                    buf.at[t],
                    buf.at[t],
                    ag_send.at[a, k],
                    ag_recv.at[a, t],
                    "tp",
                    tp_at(k) * 2 + c,
                )
            )
        launch(remote(buf.at[t], buf.at[t], ag_send.at[a, 0], ag_recv.at[a, t], "tp", peer))

    def gather_wait(a, buf, slot):
        remote(
            buf.at[slot], buf.at[slot], ag_send.at[a, 0], ag_recv.at[a, slot], "tp", peer
        ).wait_recv()

    def gather_forward(a, buf):
        for k in range(1, X):
            slot = tp_from(k) * 2 + c
            gather_wait(a, buf, slot)
            launch(
                remote(
                    buf.at[slot],
                    buf.at[slot],
                    ag_send.at[a, X - 1 + k],
                    ag_recv.at[a, slot],
                    "tp",
                    peer,
                )
            )

    def gather_finish(a, buf):
        gather_forward(a, buf)
        for k in range(X):
            gather_wait(a, buf, tp_from(k) * 2 + other)

    def project_source(layer, at):
        rows = xs[pl.ds(2 * at, 2)].reshape(2 * Rs, D)

        def one(j, carry):
            kv[j, at] = mm(rows, wkv[j]).astype(BF)
            return carry

        lax.fori_loop(2 * layer, 2 * layer + 2, one, 0)

    def send_queries(layer):
        load_q[layer].wait()
        rows = xt[layer].reshape(T, D)
        qall[layer, s] = mm(rows, wq[layer]).astype(BF)
        for i in range(1, S):
            launch(
                remote(
                    qall.at[layer, s],
                    qall.at[layer, s],
                    q_send.at[layer, i],
                    q_recv.at[layer, s],
                    "sp",
                    sp_at(i),
                )
            )

    def attend_block(layer, block, sums, stats):
        lanes = lax.broadcasted_iota(jnp.int32, (T, LANES), 1)
        packed = jnp.zeros((T, LANES), F32)
        for h in range(heads):
            cols = slice(h * HD, (h + 1) * HD)
            query = qall[layer, block, :, cols]
            keys = kv[2 * layer, :, :, cols].reshape(n * Rs, HD)
            values = kv[2 * layer + 1, :, :, cols].reshape(n * Rs, HD)
            scores = (
                lax.dot_general(query, keys, (((1,), (1,)), ((), ())), preferred_element_type=F32)
                * scale
            )
            top = jnp.max(scores, axis=-1, keepdims=True)
            raised = jnp.exp(scores - top)
            total = jnp.sum(raised, axis=-1, keepdims=True)
            sums[:, cols] = mm(raised.astype(BF), values).astype(BF)
            packed = jnp.where(lanes == 2 * h, top, packed)
            packed = jnp.where(lanes == 2 * h + 1, total, packed)
        stats[...] = packed.T[:STAT_ROWS]

    def sums_copy(layer, i, slot, block):
        return remote(
            osend.at[layer, i],
            orecv.at[layer, slot],
            r_send.at[layer, i],
            r_recv.at[layer, slot],
            "sp",
            block,
        )

    def stats_copy(layer, i, slot, block):
        return remote(
            ssend.at[layer, i],
            srecv.at[layer, slot],
            s_send.at[layer, i],
            s_recv.at[layer, slot],
            "sp",
            block,
        )

    def attend(layer, meanwhile):
        attend_block(layer, s, orecv.at[layer, s], srecv.at[layer, s])

        def one(i, carry):
            block = sp_at(i)
            remote(
                qall.at[layer, block],
                qall.at[layer, block],
                q_send.at[layer, 0],
                q_recv.at[layer, block],
                "sp",
                block,
            ).wait_recv()
            attend_block(layer, block, osend.at[layer, i], ssend.at[layer, i])
            sums_copy(layer, i, s, block).start()
            stats_copy(layer, i, s, block).start()
            return carry

        lax.fori_loop(1, S, one, 0)
        meanwhile()
        for i in range(1, S):
            block = sp_at(i)
            pending.append(sums_copy(layer, i, s, block))
            pending.append(stats_copy(layer, i, s, block))
            sums_copy(layer, i, block, block).wait_recv()
            stats_copy(layer, i, block, block).wait_recv()
        rows = srecv[layer].reshape(S * STAT_ROWS, T)
        if S * STAT_ROWS < LANES:
            rows = jnp.concatenate([rows, jnp.zeros((LANES - S * STAT_ROWS, T), F32)], axis=0)
        stats = rows.T
        for h in range(heads):
            cols = slice(h * HD, (h + 1) * HD)
            tops = [stats[:, b * STAT_ROWS + 2 * h :][:, :1] for b in range(S)]
            highest = functools.reduce(jnp.maximum, tops)
            total = jnp.zeros((T, 1), F32)
            summed = jnp.zeros((T, HD), F32)
            for b in range(S):
                factor = jnp.exp(tops[b] - highest)
                total = total + factor * stats[:, b * STAT_ROWS + 2 * h + 1 :][:, :1]
                summed = summed + factor * orecv[layer, b, :, cols].astype(F32)
            att[:, cols] = (summed / total).astype(BF)
        load_o[layer].wait()
        spread_sum(layer, att, wo.at[layer])

    def spread_sum(a, lhs, weight):
        def one(j, carry):
            cols = pl.ds(pl.multiple_of(j * TILE, TILE), TILE)
            pf[:, :, cols] = mm(lhs[...], weight[:, cols]).reshape(n, Rt, TILE)
            return carry

        lax.fori_loop(0, D // TILE, one, 0)
        order = [*range(1, X), 0]

        def first(k):
            return remote(
                p1s.at[a, k], p1r.at[a, k], p1_send.at[a, k], p1_recv.at[a, k], "tp", peer
            )

        def second(k):
            return remote(
                p2s.at[a, k],
                p2r.at[a, k],
                p2_send.at[a, k],
                p2_recv.at[a, k],
                "tp",
                tp_at(k) * 2 + c,
            )

        for k in order:
            p1s[a, k] = pf[tp_at(k) * 2 + other].astype(BF)
            launch(first(k))
        for k in range(1, X):
            first(k).wait_recv()
            p2s[a, k] = (pf[tp_at(k) * 2 + c] + p1r[a, k].astype(F32)).astype(BF)
            launch(second(k))
        first(0).wait_recv()
        own = pf[t] + p1r[a, 0].astype(F32)
        for k in range(1, X):
            second(k).wait_recv()
            own = own + p2r[a, k].astype(F32)
        residual[...] = residual[...] + own

    load_t.wait()
    residual[...] = tv[...].astype(F32)
    xt[0, t] = normed_rows(residual[...], attend_gain[0:1]).astype(BF)
    pl.semaphore_wait(barrier, X + S - 1)
    gather_start(0, xt.at[0])
    load_s.wait()
    step = 32

    def norm_source(j, carry):
        rows = pl.ds(pl.multiple_of(j * step, step), step)
        xs[t, rows] = normed_rows(sv[rows].astype(F32), source_gain[...]).astype(BF)
        return carry

    lax.fori_loop(0, Rs // step, norm_source, 0)
    gather_start(3, xs)
    gather_finish(0, xt.at[0])
    send_queries(0)
    for copy in load_kv[0]:
        copy.wait()
    gather_wait(3, xs, peer)
    project_source(0, x)
    for copy in load_kv[1]:
        copy.wait()
    project_source(1, x)
    gather_forward(3, xs)
    for k in range(1, X):
        gather_wait(3, xs, tp_from(k) * 2 + other)
        project_source(0, tp_from(k))

    def rest_of_source():
        for k in range(1, X):
            project_source(1, tp_from(k))

    attend(0, rest_of_source)
    xt[1, t] = normed_rows(residual[...], attend_gain[1:2]).astype(BF)
    gather_start(1, xt.at[1])
    gather_finish(1, xt.at[1])
    send_queries(1)
    attend(1, lambda: None)
    xt[2, t] = normed_rows(residual[...], mixer_gain[...]).astype(BF)
    gather_start(2, xt.at[2])
    gather_finish(2, xt.at[2])
    load_m[0].wait()
    load_m[1].wait()
    mixed = xt[2].reshape(T, D)
    for pad, weight, number in ((gpad, wg, 0), (upad, wu, 1)):
        lifted = mm(mixed, weight[...]).astype(BF).astype(F32)
        pad[8:] = lifted
        hs[number] = lifted[T - 8 :]
    halo_out = remote(hs, hr, h_send, h_recv, "sp", lax.rem(s + 1, S))

    @pl.when(s < S - 1)
    def _():
        halo_out.start()

    @pl.when(s == 0)
    def _():
        gpad[:8] = jnp.zeros((8, F), F32)
        upad[:8] = jnp.zeros((8, F), F32)

    @pl.when(s > 0)
    def _():
        halo_out.wait_recv()
        gpad[:8] = hr[0]
        upad[:8] = hr[1]

    @pl.when(s < S - 1)
    def _():
        halo_out.wait_send()

    def convolved(pad, taps):
        return (
            taps[0:1] * pad[6 : 6 + T] + taps[1:2] * pad[7 : 7 + T] + taps[2:3] * pad[8 : 8 + T]
        )

    gate = convolved(gpad, gate_taps)
    hid[...] = (gate / (1.0 + jnp.exp(-gate)) * convolved(upad, up_taps)).astype(BF)
    load_m[2].wait()
    spread_sum(2, hid, wd)
    result[...] = normed_rows(residual[...], final_gain[...]).astype(BF)
    for copy in pending:
        copy.wait_send()


def body(n, S, *arrays):
    (
        source,
        target,
        source_gain,
        attend_gain,
        query_weight,
        key_weight,
        value_weight,
        out_weight,
        mixer_gain,
        gate_weight,
        up_weight,
        gate_taps,
        up_taps,
        down_weight,
        final_gain,
    ) = arrays
    Rs, D = source.shape
    Rt = target.shape[0]
    W = query_weight.shape[2]
    F = gate_weight.shape[1]
    T = n * Rt
    X = n // 2
    hbm = pl.BlockSpec(memory_space=pl.ANY)
    vmem = pl.BlockSpec(memory_space=pltpu.VMEM)
    dma = pltpu.SemaphoreType.DMA
    scratch = [
        pltpu.VMEM((Rs, D), BF),
        pltpu.VMEM((Rt, D), BF),
        pltpu.VMEM((2, D, W), BF),
        pltpu.VMEM((4, D, W), BF),
        pltpu.VMEM((2, W, D), BF),
        pltpu.VMEM((D, F), BF),
        pltpu.VMEM((D, F), BF),
        pltpu.VMEM((F, D), BF),
        pltpu.VMEM((n, Rs, D), BF),
        pltpu.VMEM((3, n, Rt, D), BF),
        pltpu.VMEM((4, X, 2 * Rs, W), BF),
        pltpu.VMEM((2, S, T, W), BF),
        pltpu.VMEM((2, S, T, W), BF),
        pltpu.VMEM((2, S, T, W), BF),
        pltpu.VMEM((2, S, STAT_ROWS, T), F32),
        pltpu.VMEM((2, S, STAT_ROWS, T), F32),
        pltpu.VMEM((n, Rt, D), F32),
        pltpu.VMEM((T, W), BF),
        pltpu.VMEM((3, X, Rt, D), BF),
        pltpu.VMEM((3, X, Rt, D), BF),
        pltpu.VMEM((3, X, Rt, D), BF),
        pltpu.VMEM((3, X, Rt, D), BF),
        pltpu.VMEM((2, 8, F), F32),
        pltpu.VMEM((2, 8, F), F32),
        pltpu.VMEM((T + 8, F), F32),
        pltpu.VMEM((T + 8, F), F32),
        pltpu.VMEM((T, F), BF),
        pltpu.VMEM((Rt, D), F32),
        dma((2,)),
        dma((11,)),
        dma((4, n)),
        dma((4, n)),
        dma((2, S)),
        dma((2, S)),
        dma((2, S)),
        dma((2, S)),
        dma((2, S)),
        dma((2, S)),
        dma((3, X)),
        dma((3, X)),
        dma((3, X)),
        dma((3, X)),
        dma,
        dma,
    ]
    return pl.pallas_call(
        functools.partial(kernel, n, S),
        out_shape=jax.ShapeDtypeStruct((Rt, D), BF),
        in_specs=[
            hbm,
            hbm,
            vmem,
            vmem,
            hbm,
            hbm,
            hbm,
            hbm,
            vmem,
            hbm,
            hbm,
            vmem,
            vmem,
            hbm,
            vmem,
        ],
        out_specs=vmem,
        scratch_shapes=scratch,
        compiler_params=pltpu.CompilerParams(
            collective_id=0, has_side_effects=True, vmem_limit_bytes=67043328
        ),
    )(
        source,
        target,
        source_gain.reshape(1, D),
        attend_gain,
        query_weight,
        key_weight,
        value_weight,
        out_weight,
        mixer_gain.reshape(1, D),
        gate_weight,
        up_weight,
        gate_taps,
        up_taps,
        down_weight,
        final_gain.reshape(1, D),
    )


def solution(mesh):
    placed = (
        P(("grp", "sp", "tp"), None),
        P(("grp", "sp", "tp"), None),
        P(),
        P(),
        P(None, None, "tp"),
        P(None, None, "tp"),
        P(None, None, "tp"),
        P(None, "tp", None),
        P(),
        P(None, "tp"),
        P(None, "tp"),
        P(None, "tp"),
        P(None, "tp"),
        P("tp", None),
        P(),
    )
    return jax.shard_map(
        functools.partial(body, mesh.shape["tp"], mesh.shape["sp"]),
        mesh=mesh,
        in_specs=placed,
        out_specs=P(("grp", "sp", "tp"), None),
        check_vma=False,
    )
```

time: 303 us -> 116 us (0.38)
  waiting for transfers between devices: 138 us -> 0 us
  Pallas kernels: 0 us -> 105 us
  blocking collectives: 79 us -> 0 us
  matrix products: 33.5 us -> 0 us
  other arithmetic: 16.3 us -> 0 us
  between operations: 13.8 us -> 0.01 us
  local copies, waits for them, and re-layouts: 18.1 us -> 9.15 us
  starting transfers between devices: 3.69 us -> 0 us
    pallas_call x0 -> x1, Pallas kernels: none -> 105 us  [body(): pl.pallas_call(functools.partial(kernel, n, S), out_shape=jax.ShapeDtypeS...]
    unnamed x12 -> x0, waiting for transfers between devices: 67.5 us -> none
    reduce_scatter x3 -> x0, waiting for transfers between devices: 62.1 us -> none  [the longest x2 38.7 us: attend_layer(): lax.psum_scatter(jnp.dot(attended, w_out, preferred_element_type=jnp.floa...]
    all_gather x5 -> x0, blocking collectives: 54.7 us -> none  [the longest x2 32.4 us: attend_layer(): every_query = lax.all_gather(query_block, 'sp', axis=0, tiled=True)]
    dot_general x12 -> x0, matrix products: 33.5 us -> none  [the longest x1 8.9 us: body(): jnp.dot(lax.all_gather(source_normed, 'tp', axis=0, tiled=True), joined_w...]
    pmax x2 -> x0, blocking collectives: 24.3 us -> none  [attend_layer(): highest = lax.pmax(jnp.max(scores, axis=-1), 'sp')]
    reduce_sum x7 -> x0, other arithmetic: 8.64 us -> none  [the longest x5 4.73 us: normed_rows(): jnp.mean(wide * wide, axis=-1, keepdims=True) + EPS]
    ppermute x1 -> x0, waiting for transfers between devices: 8.04 us -> none  [shifted(): lax.ppermute(value, axis, [(source, source + steps) for source in range(f...]
  transfers between devices with their start and end apart: 9 -> 0, of which waited for: 8 -> 0; matrix products, arithmetic and copies ran while one was open for 7% -> 0% of each run, Pallas kernels for 0% -> 0%
where the time goes in v1:
time: 116 us; the launch traced here: 115 us
  Pallas kernels  105 us (91%)
  local copies, waits for them, and re-layouts  9.15 us (8%)
    pallas_call x1, Pallas kernels, body(): pl.pallas_call(functools.partial(kernel, n, S), out_shape=jax.ShapeDtypeS...  105 us
    unnamed x5, local copies, waits for them, and re-layouts  9.15 us

profile of v1, /device:TPU:0, one launch (start us, length us, event | category | flops | bytes accessed | tf_op | source)
XLA Modules:
  0.0 114.6 jit_solution(11409316461872897717)
XLA Ops:
  0.0 0.0 copy-start
  0.0 4.7 %copy.16.gate_weight = bf16[2048,704]{1,0:T(8,128)(2,1)} copy(bf16[2048,704]{0,1:T(8,128)(2,1)} %param.24) | data formatting | bytes 5767168 | tf_op args[9]
  4.8 0.0 copy-done
  4.8 2.8 %copy.17.up_weight = bf16[2048,704]{1,0:T(8,128)(2,1)} copy(bf16[2048,704]{0,1:T(8,128)(2,1)S(1)} %copy-done) | data formatting | bytes 5767168 | tf_op args[10]
  7.6 105.5 %shard_map.145 = bf16[32,2048]{1,0:T(8,128)(2,1)} custom-call(bf16[128,2048]{1,0:T(8,128)(2,1)} %source.1, bf16[32,2048]{1,0:T(8,128)(2,1)} %target.1, f32[1,2048]{1,0:T(1,128)} %bitcast.3, f32[2,2048]{1,0:T(2,128)} %attend_gain.1, bf16[2,2048,512]{2,1,0:T(8,128)(2,1)} %query_weight.1, bf16[2,2048,512]{2,1,0:T(8,128)(2,1)} %key_weight.1, ...), custom_call_target="tpu_custom_call" | custom-call | tf_op jit(solution)/shard_map/pallas_call | solution.py:505
  113.1 1.6 %copy.19 = bf16[32,2048]{1,0:T(8,128)(2,1)} copy(bf16[32,2048]{1,0:T(8,128)(2,1)} %shard_map.145) | data formatting | bytes 262144
Async XLA Ops:
  0.0 4.8 %copy-start = (bf16[2048,704]{0,1:T(8,128)(2,1)S(1)}, bf16[2048,704]{0,1:T(8,128)(2,1)}, u32[]{:S(2)}) copy-start(bf16[2048,704]{0,1:T(8,128)(2,1)} %param.25) | copy-start | bytes 8650756

commit v2 on v1

--- a/solution.py
+++ b/solution.py
@@ -95,7 +95,7 @@
     W = wq.shape[2]
     T = n * Rt
     heads = W // HD
-    F = wg.shape[1]
+    F = wg.shape[0]
     scale = HD ** (-0.5)
     t = lax.axis_index("tp")
     s = lax.axis_index("sp")
@@ -207,21 +207,28 @@
 
         lax.fori_loop(2 * layer, 2 * layer + 2, one, 0)
 
+    def has_next(way, where):
+        return where < S - 1 if way == 0 else where > 0
+
+    def query_copy(layer, way, block):
+        return remote(
+            qall.at[layer, block],
+            qall.at[layer, block],
+            q_send.at[layer, way, block],
+            q_recv.at[layer, block],
+            "sp",
+            jnp.clip(s + 1 - 2 * way, 0, S - 1),
+        )
+
     def send_queries(layer):
         load_q[layer].wait()
         rows = xt[layer].reshape(T, D)
         qall[layer, s] = mm(rows, wq[layer]).astype(BF)
-        for i in range(1, S):
-            launch(
-                remote(
-                    qall.at[layer, s],
-                    qall.at[layer, s],
-                    q_send.at[layer, i],
-                    q_recv.at[layer, s],
-                    "sp",
-                    sp_at(i),
-                )
-            )
+        for way in range(2):
+
+            @pl.when(has_next(way, s))
+            def _():
+                query_copy(layer, way, s).start()
 
     def attend_block(layer, block, sums, stats):
         lanes = lax.broadcasted_iota(jnp.int32, (T, LANES), 1)
@@ -267,28 +274,38 @@
         attend_block(layer, s, orecv.at[layer, s], srecv.at[layer, s])
 
         def one(i, carry):
-            block = sp_at(i)
-            remote(
-                qall.at[layer, block],
-                qall.at[layer, block],
-                q_send.at[layer, 0],
-                q_recv.at[layer, block],
-                "sp",
-                block,
-            ).wait_recv()
-            attend_block(layer, block, osend.at[layer, i], ssend.at[layer, i])
-            sums_copy(layer, i, s, block).start()
-            stats_copy(layer, i, s, block).start()
+            for way in range(2):
+                block = s - i if way == 0 else s + i
+
+                @pl.when(block >= 0 if way == 0 else block < S)
+                def _():
+                    query_copy(layer, way, block).wait_recv()
+
+                    @pl.when(has_next(way, s))
+                    def _():
+                        query_copy(layer, way, block).start()
+
+            for way in range(2):
+                block = s - i if way == 0 else s + i
+
+                @pl.when(block >= 0 if way == 0 else block < S)
+                def _():
+                    attend_block(layer, block, osend.at[layer, block], ssend.at[layer, block])
+                    sums_copy(layer, block, s, block).start()
+                    stats_copy(layer, block, s, block).start()
+
             return carry
 
         lax.fori_loop(1, S, one, 0)
         meanwhile()
-        for i in range(1, S):
+
+        def wait_block(i, carry):
             block = sp_at(i)
-            pending.append(sums_copy(layer, i, s, block))
-            pending.append(stats_copy(layer, i, s, block))
-            sums_copy(layer, i, block, block).wait_recv()
-            stats_copy(layer, i, block, block).wait_recv()
+            sums_copy(layer, block, block, block).wait_recv()
+            stats_copy(layer, block, block, block).wait_recv()
+            return carry
+
+        lax.fori_loop(1, S, wait_block, 0)
         rows = srecv[layer].reshape(S * STAT_ROWS, T)
         if S * STAT_ROWS < LANES:
             rows = jnp.concatenate([rows, jnp.zeros((LANES - S * STAT_ROWS, T), F32)], axis=0)
@@ -391,7 +408,13 @@
     load_m[1].wait()
     mixed = xt[2].reshape(T, D)
     for pad, weight, number in ((gpad, wg, 0), (upad, wu, 1)):
-        lifted = mm(mixed, weight[...]).astype(BF).astype(F32)
+        lifted = (
+            lax.dot_general(
+                mixed, weight[...], (((1,), (1,)), ((), ())), preferred_element_type=F32
+            )
+            .astype(BF)
+            .astype(F32)
+        )
         pad[8:] = lifted
         hs[number] = lifted[T - 8 :]
     halo_out = remote(hs, hr, h_send, h_recv, "sp", lax.rem(s + 1, S))
@@ -427,6 +450,23 @@
     result[...] = normed_rows(residual[...], final_gain[...]).astype(BF)
     for copy in pending:
         copy.wait_send()
+    for layer in range(2):
+
+        def wait_sent(block, carry):
+            for way in range(2):
+
+                @pl.when(has_next(way, s) & (block <= s if way == 0 else block >= s))
+                def _():
+                    query_copy(layer, way, block).wait_send()
+
+            @pl.when(block != s)
+            def _():
+                sums_copy(layer, block, s, block).wait_send()
+                stats_copy(layer, block, s, block).wait_send()
+
+            return carry
+
+        lax.fori_loop(0, S, wait_sent, 0)
 
 
 def body(n, S, *arrays):
@@ -462,8 +502,8 @@
         pltpu.VMEM((2, D, W), BF),
         pltpu.VMEM((4, D, W), BF),
         pltpu.VMEM((2, W, D), BF),
-        pltpu.VMEM((D, F), BF),
-        pltpu.VMEM((D, F), BF),
+        pltpu.VMEM((F, D), BF),
+        pltpu.VMEM((F, D), BF),
         pltpu.VMEM((F, D), BF),
         pltpu.VMEM((n, Rs, D), BF),
         pltpu.VMEM((3, n, Rt, D), BF),
@@ -489,7 +529,7 @@
         dma((11,)),
         dma((4, n)),
         dma((4, n)),
-        dma((2, S)),
+        dma((2, 2, S)),
         dma((2, S)),
         dma((2, S)),
         dma((2, S)),
@@ -537,8 +577,8 @@
         value_weight,
         out_weight,
         mixer_gain.reshape(1, D),
-        gate_weight,
-        up_weight,
+        gate_weight.T,
+        up_weight.T,
         gate_taps,
         up_taps,
         down_weight,

time: 116 us -> 115 us (level)
  Pallas kernels: 105 us -> 113 us
  local copies, waits for them, and re-layouts: 9.15 us -> 1.57 us
    unnamed x5 -> x1, local copies, waits for them, and re-layouts: 9.15 us -> 1.57 us
    pallas_call x1, Pallas kernels: 105 us -> 113 us  [body(): pl.pallas_call(functools.partial(kernel, n, S), out_shape=jax.ShapeDtypeS...]
where the time goes in v2:
time: 115 us; the launch traced here: 114 us
  Pallas kernels  113 us (98%)
  local copies, waits for them, and re-layouts  1.57 us (1%)
    pallas_call x1, Pallas kernels, body(): pl.pallas_call(functools.partial(kernel, n, S), out_shape=jax.ShapeDtypeS...  113 us

profile of v2, /device:TPU:0, one launch (start us, length us, event | category | flops | bytes accessed | tf_op | source)
XLA Modules:
  0.0 114.2 jit_solution(16874617549782447917)
XLA Ops:
  0.0 112.7 %shard_map.145 = bf16[32,2048]{1,0:T(8,128)(2,1)} custom-call(bf16[128,2048]{1,0:T(8,128)(2,1)} %source.1, bf16[32,2048]{1,0:T(8,128)(2,1)} %target.1, f32[1,2048]{1,0:T(1,128)} %bitcast.7, f32[2,2048]{1,0:T(2,128)} %attend_gain.1, bf16[2,2048,512]{2,1,0:T(8,128)(2,1)} %query_weight.1, bf16[2,2048,512]{2,1,0:T(8,128)(2,1)} %key_weight.1, ...), custom_call_target="tpu_custom_call" | custom-call | tf_op jit(solution)/shard_map/pallas_call | solution.py:545
  112.7 1.6 %copy.17 = bf16[32,2048]{1,0:T(8,128)(2,1)} copy(bf16[32,2048]{1,0:T(8,128)(2,1)} %shard_map.145) | data formatting | bytes 262144

commit v3 on v2

--- a/solution.py
+++ b/solution.py
@@ -156,8 +156,7 @@
         pltpu.make_async_copy(up_weight, wu, w_sem.at[9]),
         pltpu.make_async_copy(down_weight, wd, w_sem.at[10]),
     ]
-    for copy in [load_q[0], *load_kv[0], *load_kv[1], load_o[0], load_q[1], load_o[1], *load_m]:
-        copy.start()
+    load_q[0].start()
 
     def gather_start(a, buf):
         for k in range(1, X):
@@ -207,28 +206,22 @@
 
         lax.fori_loop(2 * layer, 2 * layer + 2, one, 0)
 
-    def has_next(way, where):
-        return where < S - 1 if way == 0 else where > 0
-
-    def query_copy(layer, way, block):
+    def query_copy(layer, i, block, where):
         return remote(
             qall.at[layer, block],
             qall.at[layer, block],
-            q_send.at[layer, way, block],
+            q_send.at[layer, i],
             q_recv.at[layer, block],
             "sp",
-            jnp.clip(s + 1 - 2 * way, 0, S - 1),
+            where,
         )
 
     def send_queries(layer):
         load_q[layer].wait()
         rows = xt[layer].reshape(T, D)
         qall[layer, s] = mm(rows, wq[layer]).astype(BF)
-        for way in range(2):
-
-            @pl.when(has_next(way, s))
-            def _():
-                query_copy(layer, way, s).start()
+        for i in range(1, S):
+            launch(query_copy(layer, i, s, sp_at(i)))
 
     def attend_block(layer, block, sums, stats):
         lanes = lax.broadcasted_iota(jnp.int32, (T, LANES), 1)
@@ -274,26 +267,11 @@
         attend_block(layer, s, orecv.at[layer, s], srecv.at[layer, s])
 
         def one(i, carry):
-            for way in range(2):
-                block = s - i if way == 0 else s + i
-
-                @pl.when(block >= 0 if way == 0 else block < S)
-                def _():
-                    query_copy(layer, way, block).wait_recv()
-
-                    @pl.when(has_next(way, s))
-                    def _():
-                        query_copy(layer, way, block).start()
-
-            for way in range(2):
-                block = s - i if way == 0 else s + i
-
-                @pl.when(block >= 0 if way == 0 else block < S)
-                def _():
-                    attend_block(layer, block, osend.at[layer, block], ssend.at[layer, block])
-                    sums_copy(layer, block, s, block).start()
-                    stats_copy(layer, block, s, block).start()
-
+            block = sp_at(i)
+            query_copy(layer, 0, block, block).wait_recv()
+            attend_block(layer, block, osend.at[layer, block], ssend.at[layer, block])
+            sums_copy(layer, block, s, block).start()
+            stats_copy(layer, block, s, block).start()
             return carry
 
         lax.fori_loop(1, S, one, 0)
@@ -367,6 +345,8 @@
     xt[0, t] = normed_rows(residual[...], attend_gain[0:1]).astype(BF)
     pl.semaphore_wait(barrier, X + S - 1)
     gather_start(0, xt.at[0])
+    for copy in load_kv[0]:
+        copy.start()
     load_s.wait()
     step = 32
 
@@ -379,6 +359,8 @@
     gather_start(3, xs)
     gather_finish(0, xt.at[0])
     send_queries(0)
+    for copy in [*load_kv[1], load_o[0], load_q[1], load_o[1]]:
+        copy.start()
     for copy in load_kv[0]:
         copy.wait()
     gather_wait(3, xs, peer)
@@ -386,6 +368,8 @@
     for copy in load_kv[1]:
         copy.wait()
     project_source(1, x)
+    for copy in load_m:
+        copy.start()
     gather_forward(3, xs)
     for k in range(1, X):
         gather_wait(3, xs, tp_from(k) * 2 + other)
@@ -452,21 +436,13 @@
         copy.wait_send()
     for layer in range(2):
 
-        def wait_sent(block, carry):
-            for way in range(2):
-
-                @pl.when(has_next(way, s) & (block <= s if way == 0 else block >= s))
-                def _():
-                    query_copy(layer, way, block).wait_send()
-
-            @pl.when(block != s)
-            def _():
-                sums_copy(layer, block, s, block).wait_send()
-                stats_copy(layer, block, s, block).wait_send()
-
+        def wait_sent(i, carry):
+            block = sp_at(i)
+            sums_copy(layer, block, s, block).wait_send()
+            stats_copy(layer, block, s, block).wait_send()
             return carry
 
-        lax.fori_loop(0, S, wait_sent, 0)
+        lax.fori_loop(1, S, wait_sent, 0)
 
 
 def body(n, S, *arrays):
@@ -529,7 +505,7 @@
         dma((11,)),
         dma((4, n)),
         dma((4, n)),
-        dma((2, 2, S)),
+        dma((2, S)),
         dma((2, S)),
         dma((2, S)),
         dma((2, S)),

time: 115 us -> 104 us (0.904); the launches traced: 114 us -> 102 us
  Pallas kernels: 113 us -> 100 us
    pallas_call x1, Pallas kernels: 113 us -> 100 us  [body(): pl.pallas_call(functools.partial(kernel, n, S), out_shape=jax.ShapeDtypeS...]
where the time goes in v3:
time: 104 us; the launch traced here: 102 us
  Pallas kernels  100 us (96%)
  local copies, waits for them, and re-layouts  1.57 us (2%)
    pallas_call x1, Pallas kernels, body(): pl.pallas_call(functools.partial(kernel, n, S), out_shape=jax.ShapeDtypeS...  100 us

profile of v3, /device:TPU:0, one launch (start us, length us, event | category | flops | bytes accessed | tf_op | source)
XLA Modules:
  0.0 102.0 jit_solution(3947181063145994215)
XLA Ops:
  0.0 100.4 %shard_map.145 = bf16[32,2048]{1,0:T(8,128)(2,1)} custom-call(bf16[128,2048]{1,0:T(8,128)(2,1)} %source.1, bf16[32,2048]{1,0:T(8,128)(2,1)} %target.1, f32[1,2048]{1,0:T(1,128)} %bitcast.7, f32[2,2048]{1,0:T(2,128)} %attend_gain.1, bf16[2,2048,512]{2,1,0:T(8,128)(2,1)} %query_weight.1, bf16[2,2048,512]{2,1,0:T(8,128)(2,1)} %key_weight.1, ...), custom_call_target="tpu_custom_call" | custom-call | tf_op jit(solution)/shard_map/pallas_call | solution.py:521
  100.4 1.6 %copy.17 = bf16[32,2048]{1,0:T(8,128)(2,1)} copy(bf16[32,2048]{1,0:T(8,128)(2,1)} %shard_map.145) | data formatting | bytes 262144

commit v4 on v3

--- a/solution.py
+++ b/solution.py
@@ -391,7 +391,19 @@
     load_m[0].wait()
     load_m[1].wait()
     mixed = xt[2].reshape(T, D)
-    for pad, weight, number in ((gpad, wg, 0), (upad, wu, 1)):
+    pads = ((gpad, wg), (upad, wu))
+
+    def halo_out(number):
+        return remote(
+            hs.at[number],
+            hr.at[number],
+            h_send.at[number],
+            h_recv.at[number],
+            "sp",
+            lax.rem(s + 1, S),
+        )
+
+    for number, (pad, weight) in enumerate(pads):
         lifted = (
             lax.dot_general(
                 mixed, weight[...], (((1,), (1,)), ((), ())), preferred_element_type=F32
@@ -399,36 +411,44 @@
             .astype(BF)
             .astype(F32)
         )
+        hs[number] = lifted[T - 8 :]
+
+        @pl.when(s < S - 1)
+        def _():
+            halo_out(number).start()
+
         pad[8:] = lifted
-        hs[number] = lifted[T - 8 :]
-    halo_out = remote(hs, hr, h_send, h_recv, "sp", lax.rem(s + 1, S))
+
+    def hidden_rows(start, stop):
+        def convolved(pad, taps):
+            return (
+                taps[0:1] * pad[6 + start : 6 + stop]
+                + taps[1:2] * pad[7 + start : 7 + stop]
+                + taps[2:3] * pad[8 + start : 8 + stop]
+            )
+
+        gate = convolved(gpad, gate_taps)
+        hid[start:stop] = (gate / (1.0 + jnp.exp(-gate)) * convolved(upad, up_taps)).astype(BF)
+
+    hidden_rows(16, T)
+
+    @pl.when(s == 0)
+    def _():
+        for pad, _weight in pads:
+            pad[:8] = jnp.zeros((8, F), F32)
+
+    @pl.when(s > 0)
+    def _():
+        for number, (pad, _weight) in enumerate(pads):
+            halo_out(number).wait_recv()
+            pad[:8] = hr[number]
 
     @pl.when(s < S - 1)
     def _():
-        halo_out.start()
-
-    @pl.when(s == 0)
-    def _():
-        gpad[:8] = jnp.zeros((8, F), F32)
-        upad[:8] = jnp.zeros((8, F), F32)
-
-    @pl.when(s > 0)
-    def _():
-        halo_out.wait_recv()
-        gpad[:8] = hr[0]
-        upad[:8] = hr[1]
-
-    @pl.when(s < S - 1)
-    def _():
-        halo_out.wait_send()
-
-    def convolved(pad, taps):
-        return (
-            taps[0:1] * pad[6 : 6 + T] + taps[1:2] * pad[7 : 7 + T] + taps[2:3] * pad[8 : 8 + T]
-        )
-
-    gate = convolved(gpad, gate_taps)
-    hid[...] = (gate / (1.0 + jnp.exp(-gate)) * convolved(upad, up_taps)).astype(BF)
+        for number in range(2):
+            halo_out(number).wait_send()
+
+    hidden_rows(0, 16)
     load_m[2].wait()
     spread_sum(2, hid, wd)
     result[...] = normed_rows(residual[...], final_gain[...]).astype(BF)
@@ -515,8 +535,8 @@
         dma((3, X)),
         dma((3, X)),
         dma((3, X)),
-        dma,
-        dma,
+        dma((2,)),
+        dma((2,)),
     ]
     return pl.pallas_call(
         functools.partial(kernel, n, S),

time: 104 us -> 104 us (level)
  no operation moved by 1% of the time
where the time goes in v4:
time: 104 us; the launch traced here: 102 us
  Pallas kernels  100 us (96%)
  local copies, waits for them, and re-layouts  1.57 us (2%)
    pallas_call x1, Pallas kernels, body(): pl.pallas_call(functools.partial(kernel, n, S), out_shape=jax.ShapeDtypeS...  100 us

profile of v4, /device:TPU:0, one launch (start us, length us, event | category | flops | bytes accessed | tf_op | source)
XLA Modules:
  0.0 102.0 jit_solution(15526519098898153407)
XLA Ops:
  0.0 100.4 %shard_map.145 = bf16[32,2048]{1,0:T(8,128)(2,1)} custom-call(bf16[128,2048]{1,0:T(8,128)(2,1)} %source.1, bf16[32,2048]{1,0:T(8,128)(2,1)} %target.1, f32[1,2048]{1,0:T(1,128)} %bitcast.7, f32[2,2048]{1,0:T(2,128)} %attend_gain.1, bf16[2,2048,512]{2,1,0:T(8,128)(2,1)} %query_weight.1, bf16[2,2048,512]{2,1,0:T(8,128)(2,1)} %key_weight.1, ...), custom_call_target="tpu_custom_call" | custom-call | tf_op jit(solution)/shard_map/pallas_call | solution.py:541
  100.4 1.6 %copy.17 = bf16[32,2048]{1,0:T(8,128)(2,1)} copy(bf16[32,2048]{1,0:T(8,128)(2,1)} %shard_map.145) | data formatting | bytes 262144
